TPU v7x, 32 devices: a whole 2x2x4 slice. The times are simulated.
32 devices in a mesh: fs: 8 (over z, y), tp: 4 (over x, core).
Axes of the slice: x: 2, y: 2, z: 4, core: 2. Of those that a mesh axis runs over, the one named last changes fastest.
Arguments:
- hidden_in: bfloat16 [2048, 2048], P('fs'), may hold values from -6 to 6
- mix_gain: float32 [2048], replicated, may hold values from 0.1 to 1.9
- value_proj: float32 [2048, 512], P('fs', 'tp'), may hold values from -0.125 to 0.125
- gate_proj: float32 [2048, 512], P('fs', 'tp'), may hold values from -0.125 to 0.125
- out_proj: float32 [2048, 512], P('fs', 'tp'), may hold values from -0.25 to 0.25
- value_scale: float32 [512], P('tp'), may hold values from 0.3 to 3
- gate_scale: float32 [512], P('tp'), may hold values from 0.5 to 2
- out_scale: float32 [2048], P('fs'), may hold values from 0.5 to 2
- conv_kernel: bfloat16 [31, 512], P(None, 'tp'), may hold values from -1 to 1
- norm_gain: float32 [512], P('tp'), may hold values from 0.1 to 1.9
- norm_shift: float32 [512], P('tp'), may hold values from -3 to 3
- mlp_gain: float32 [2048], replicated, may hold values from 0.1 to 1.9
- mlp_gate: float32 [2048, 2816], P('fs', 'tp'), may hold values from -0.125 to 0.125
- mlp_up: float32 [2048, 2816], P('fs', 'tp'), may hold values from -0.125 to 0.125
- mlp_down: float32 [2048, 2816], P('fs', 'tp'), may hold values from -0.109375 to 0.109375
- mlp_gate_scale: float32 [2816], P('tp'), may hold values from 0.5 to 2
- mlp_up_scale: float32 [2816], P('tp'), may hold values from 0.5 to 2
- mlp_down_scale: float32 [2048], P('fs'), may hold values from 0.5 to 2
Outputs:
- layer_out: bfloat16 [2048, 2048], P('fs')
All inputs are finite; a program needn't handle non-finite values.
Results may differ from a plain program's by a relative error of at most 0.019.
Values may be sent and summed in bfloat16 or wider, within the bound.
A program may use at most 64 MiB of HBM per device.

v0:
```python
import jax
import jax.numpy as jnp
from jax import lax
from jax.sharding import PartitionSpec as P


def row_norm(rows, gain):
    scale = lax.rsqrt(jnp.mean(rows * rows, axis=-1, keepdims=True) + 1e-06)
    return rows * scale * gain


def contract_last(left, right):
    return lax.dot_general(
        left, right, (((1,), (1,)), ((), ())), preferred_element_type=jnp.float32
    )


def body(
    hidden_in,
    mix_gain,
    value_proj,
    gate_proj,
    out_proj,
    value_scale,
    gate_scale,
    out_scale,
    conv_kernel,
    norm_gain,
    norm_shift,
    mlp_gain,
    mlp_gate,
    mlp_up,
    mlp_down,
    mlp_gate_scale,
    mlp_up_scale,
    mlp_down_scale,
):
    out_full, down_full = (
        lax.all_gather(out_scale, "fs", axis=0, tiled=True),
        lax.all_gather(mlp_down_scale, "fs", axis=0, tiled=True),
    )
    value_w, gate_w, out_w = (
        lax.all_gather(value_proj.astype(jnp.bfloat16), "fs", axis=0, tiled=True),
        lax.all_gather(gate_proj.astype(jnp.bfloat16), "fs", axis=0, tiled=True),
        lax.all_gather(out_proj.astype(jnp.bfloat16), "fs", axis=0, tiled=True),
    )
    mlp_shards = (
        mlp_gate.astype(jnp.bfloat16),
        mlp_up.astype(jnp.bfloat16),
        mlp_down.astype(jnp.bfloat16),
    )
    rows = hidden_in.astype(jnp.float32)
    normed = row_norm(rows, mix_gain).astype(jnp.bfloat16)
    value_pre = jnp.dot(normed, value_w, preferred_element_type=jnp.float32) * value_scale
    gate_pre = jnp.dot(normed, gate_w, preferred_element_type=jnp.float32) * gate_scale
    glu = value_pre * jax.nn.sigmoid(gate_pre)
    seq_len = glu.shape[0]
    taps = conv_kernel.shape[0]
    padded = jnp.pad(glu, ((taps - 1, 0), (0, 0)))
    kernel = conv_kernel.astype(jnp.float32)
    conved = jnp.zeros_like(glu)
    for tap in range(taps):
        conved = conved + padded[tap : tap + seq_len] * kernel[tap]
    channels = conved.shape[1] * lax.axis_size("tp")
    sums, squares = lax.psum((jnp.sum(conved, axis=1), jnp.sum(conved * conved, axis=1)), "tp")
    chan_mean = (sums / channels)[:, None]
    chan_var = (squares / channels)[:, None] - chan_mean * chan_mean
    act = jax.nn.silu(
        (conved - chan_mean) * lax.rsqrt(chan_var + 1e-05) * norm_gain + norm_shift
    ).astype(jnp.bfloat16)
    conv_term = contract_last(act, out_w) * out_full
    middle_f = (
        (rows + lax.psum(conv_term.astype(jnp.bfloat16), "tp").astype(jnp.float32))
        .astype(jnp.bfloat16)
        .astype(jnp.float32)
    )
    normed_mlp = row_norm(middle_f, mlp_gain).astype(jnp.bfloat16)
    collected = (
        lax.all_gather(mlp_shards[0], "fs", axis=0, tiled=True),
        lax.all_gather(mlp_shards[1], "fs", axis=0, tiled=True),
        lax.all_gather(mlp_shards[2], "fs", axis=0, tiled=True),
    )
    gate_mlp = (
        jnp.dot(normed_mlp, collected[0], preferred_element_type=jnp.float32) * mlp_gate_scale
    )
    up_mlp = jnp.dot(normed_mlp, collected[1], preferred_element_type=jnp.float32) * mlp_up_scale
    hidden_act = (jax.nn.silu(gate_mlp) * up_mlp).astype(jnp.bfloat16)
    mlp_term = contract_last(hidden_act, collected[2]) * down_full
    return (middle_f + lax.psum(mlp_term.astype(jnp.bfloat16), "tp").astype(jnp.float32)).astype(
        jnp.bfloat16
    )


def solution(mesh):
    return jax.shard_map(
        body,
        mesh=mesh,
        in_specs=(
            P("fs", None),
            P(),
            P("fs", "tp"),
            P("fs", "tp"),
            P("fs", "tp"),
            P("tp"),
            P("tp"),
            P("fs"),
            P(None, "tp"),
            P("tp"),
            P("tp"),
            P(),
            P("fs", "tp"),
            P("fs", "tp"),
            P("fs", "tp"),
            P("tp"),
            P("tp"),
            P("fs"),
        ),
        out_specs=P("fs", None),
        check_vma=False,
    )
```

profile of v0, /device:TPU:0, one launch (start us, length us, event | category | flops | bytes accessed | tf_op | source)
XLA Modules:
  0.0 370.3 jit_solution(7887861853661166801)
XLA Ops:
  7.4 0.0 all-reduce.5.cloned.1.call-start
  7.4 0.8 convert_element_type.63
  8.2 1.5 fusion.2
  9.8 0.9 convert_element_type.61
  10.7 33.0 %all_gather.24 = bf16[2048,128]{1,0:T(8,128)(2,1)S(1)} all-gather(bf16[256,128]{1,0:T(8,128)(2,1)S(1)} %convert_element_type.61), channel_id=1, replica_groups=mesh['fs'=8,'tp'=4] {'fs'}, dimensions={0}, use_global_device_ids=true | all-gather | bytes 589824 | tf_op jit(solution)/shard_map/all_gather | solution.py:43
  43.7 0.9 convert_element_type.62
  44.6 31.4 %all_gather.25 = bf16[2048,128]{1,0:T(8,128)(2,1)S(1)} all-gather(bf16[256,128]{1,0:T(8,128)(2,1)S(1)} %convert_element_type.62), channel_id=1, replica_groups=mesh['fs'=8,'tp'=4] {'fs'}, dimensions={0}, use_global_device_ids=true | all-gather | bytes 589824 | tf_op jit(solution)/shard_map/all_gather | solution.py:44
  76.0 31.3 %all_gather.26 = bf16[2048,128]{1,0:T(8,128)(2,1)S(1)} all-gather(bf16[256,128]{1,0:T(8,128)(2,1)S(1)} %convert_element_type.65), channel_id=1, replica_groups=mesh['fs'=8,'tp'=4] {'fs'}, dimensions={0}, use_global_device_ids=true | all-gather | bytes 589824 | tf_op jit(solution)/shard_map/all_gather | solution.py:45
  107.3 20.7 %all-gather = f32[8,1,256]{2,1,0:T(1,128)S(1)} all-gather(f32[1,1,256]{2,1,0:T(1,128)S(1)} %bitcast.74), channel_id=1, replica_groups=mesh['fs'=8,'tp'=4] {'fs'}, dimensions={0}, use_global_device_ids=true | all-gather | bytes 9216 | tf_op jit(solution)/shard_map/all_gather | solution.py:39
  128.1 0.5 convolution_multiply_fusion.5
  128.6 0.5 fusion.16
  129.2 0.6 fusion.91
  129.7 5.7 %all-reduce.1 = (f32[256]{0:T(256)S(1)}, f32[256]{0:T(256)S(1)}) all-reduce(f32[256]{0:T(256)S(1)} %get-tuple-element.6, f32[256]{0:T(256)S(1)} %get-tuple-element.5), channel_id=1, replica_groups=mesh['fs'=8,'tp'=4] {'tp'}, use_global_device_ids=true, to_apply=%region_4.5 | all-reduce | flops 512 | bytes 4096 | tf_op jit(solution)/shard_map/psum | solution.py:65
  135.4 1.5 fusion.1
  136.9 0.0 all-gather.6.cloned.1.call-start
  137.0 0.8 convert_element_type.71
  137.8 0.0 all-gather.6.cloned.1.call-update
  137.8 0.0 all-gather.10.cloned.1.call-start
  137.9 0.8 convert_element_type.74
  138.7 0.0 all-gather.8.cloned.1.call-start
  138.8 0.8 convert_element_type.72
  139.6 0.0 all-reduce.7.cloned.1.call-start
  139.6 16.5 %all-gather.1 = f32[8,1,256]{2,1,0:T(1,128)S(1)} all-gather(f32[1,1,256]{2,1,0:T(1,128)S(1)} %bitcast.75), channel_id=1, replica_groups=mesh['fs'=8,'tp'=4] {'fs'}, dimensions={0}, use_global_device_ids=true | all-gather | bytes 9216 | tf_op jit(solution)/shard_map/all_gather | solution.py:40
  156.2 14.7 %all-reduce.5.cloned.1.call-done = bf16[256,2048]{1,0:T(8,128)(2,1)} async-done(((bf16[256,2048]{1,0:T(8,128)(2,1)}), bf16[256,2048]{1,0:T(8,128)(2,1)}) %all-reduce.5.cloned.1.call-update) | async-done | bytes 1048592 | tf_op jit(solution)/shard_map/psum | solution.py:73
  170.9 1.8 fusion.6
  172.6 24.8 %all-gather.6.cloned.1.call-done = bf16[2048,704]{0,1:T(8,128)(2,1)} async-done(((bf16[256,704]{0,1:T(8,128)(2,1)}), bf16[2048,704]{0,1:T(8,128)(2,1)}) %all-gather.6.cloned.1.call-update) | async-done | bytes 2883600 | tf_op jit(solution)/shard_map/all_gather | solution.py:79
  197.4 2.8 convolution_multiply_fusion.3
  200.3 57.6 %all-gather.10.cloned.1.call-done = bf16[2048,704]{0,1:T(8,128)(2,1)} async-done(((bf16[256,704]{0,1:T(8,128)(2,1)}), bf16[2048,704]{0,1:T(8,128)(2,1)}) %all-gather.10.cloned.1.call-update) | async-done | bytes 2883600 | tf_op jit(solution)/shard_map/all_gather | solution.py:81
  257.9 60.5 %all-gather.8.cloned.1.call-done = bf16[2048,704]{0,1:T(8,128)(2,1)} async-done(((bf16[256,704]{0,1:T(8,128)(2,1)}), bf16[2048,704]{0,1:T(8,128)(2,1)}) %all-gather.8.cloned.1.call-update) | async-done | bytes 2883600 | tf_op jit(solution)/shard_map/all_gather | solution.py:80
  318.5 7.0 %fusion = bf16[256,2048]{1,0:T(8,128)(2,1)} fusion(bf16[2048,704]{0,1:T(8,128)(2,1)} %all-gather.10.cloned.1.call-done, f32[2048]{0:T(1024)S(1)} %bitcast.73, bf16[2048,704]{0,1:T(8,128)(2,1)} %all-gather.8.cloned.1.call-done, f32[256,704]{0,1:T(8,128)S(1)} %convolution_multiply_fusion.3, f32[704]{0:T(1024)S(1)} %copy-done.10, ...), kind=kOutput, calls=%fused_computation.8 | convolution fusion | flops 1480802304 | bytes 8605440 | tf_op jit(solution)/shard_map/dot_general | solution.py:13
  325.5 34.6 %all-reduce.7.cloned.1.call-done = bf16[256,2048]{1,0:T(8,128)(2,1)} async-done(((bf16[256,2048]{1,0:T(8,128)(2,1)}), bf16[256,2048]{1,0:T(8,128)(2,1)}) %all-reduce.7.cloned.1.call-update) | async-done | bytes 1048592 | tf_op jit(solution)/shard_map/psum | solution.py:89
  360.1 2.6 fusion.9
  (40 shorter events, 0.2 us)
Async XLA Ops:
  7.4 120.7 %copy-start = (bf16[256,2048]{1,0:T(8,128)(2,1)S(1)}, bf16[256,2048]{1,0:T(8,128)(2,1)}, u32[]{:S(2)}) copy-start(bf16[256,2048]{1,0:T(8,128)(2,1)} %param.18) | copy-start | bytes 3145732
  7.4 68.6 %copy-start.4 = (f32[256,128]{1,0:T(8,128)S(1)}, f32[256,128]{1,0:T(8,128)}, u32[]{:S(2)}) copy-start(f32[256,128]{1,0:T(8,128)} %param.22) | copy-start | bytes 393220
  7.4 100.0 %copy-start.5 = (f32[256]{0:T(256)S(1)}, f32[256]{0:T(256)}, u32[]{:S(2)}) copy-start(f32[256]{0:T(256)} %param.25) | copy-start | bytes 3076
  7.4 120.7 %copy-start.7 = (f32[2048]{0:T(1024)S(1)}, f32[2048]{0:T(1024)}, u32[]{:S(2)}) copy-start(f32[2048]{0:T(1024)} %param.19) | copy-start | bytes 24580
  7.4 120.7 %copy-start.11 = (f32[128]{0:T(128)S(1)}, f32[128]{0:T(128)}, u32[]{:S(2)}) copy-start(f32[128]{0:T(128)} %param.23) | copy-start | bytes 1540
  7.4 163.5 %all-reduce.5.cloned.1.call-start = ((), (), s32[]{:S(2)}) async-start(), calls=%async_computation | async-start | bytes 2097152 | tf_op jit(solution)/shard_map/psum | solution.py:73
  43.7 84.9 %copy-start.12 = (f32[128]{0:T(128)S(1)}, f32[128]{0:T(128)}, u32[]{:S(2)}) copy-start(f32[128]{0:T(128)} %param.24) | copy-start | bytes 1540
  128.6 6.8 %copy-start.13 = (f32[128]{0:T(128)S(1)}, f32[128]{0:T(128)}, u32[]{:S(2)}) copy-start(f32[128]{0:T(128)} %param.28) | copy-start | bytes 1540
  128.6 6.8 %copy-start.14 = (f32[128]{0:T(128)S(1)}, f32[128]{0:T(128)}, u32[]{:S(2)}) copy-start(f32[128]{0:T(128)} %param.27) | copy-start | bytes 1540
  129.1 7.9 %copy-start.1 = (f32[256,704]{0,1:T(8,128)S(1)}, f32[256,704]{0,1:T(8,128)}, u32[]{:S(2)}) copy-start(f32[256,704]{0,1:T(8,128)} %param.30) | copy-start | bytes 2162692
  135.4 2.5 copy-start.2
  136.9 1.8 copy-start.3
  136.9 2.7 copy-start.6
  136.9 60.5 %all-gather.6.cloned.1.call-start = ((), (), s32[]{:S(2)}) async-start(), calls=%async_computation.1 | async-start | bytes 3244032 | tf_op jit(solution)/shard_map/all_gather | solution.py:79
  137.8 120.1 %all-gather.10.cloned.1.call-start = ((), (), s32[]{:S(2)}) async-start(), calls=%async_computation.3 | async-start | bytes 3244032 | tf_op jit(solution)/shard_map/all_gather | solution.py:81
  138.7 58.8 %copy-start.8 = (f32[2048]{0:T(1024)S(1)}, f32[2048]{0:T(1024)}, u32[]{:S(2)}) copy-start(f32[2048]{0:T(1024)} %param.29) | copy-start | bytes 24580
  138.7 58.8 %copy-start.9 = (f32[704]{0:T(1024)S(1)}, f32[704]{0:T(1024)}, u32[]{:S(2)}) copy-start(f32[704]{0:T(1024)} %param.33) | copy-start | bytes 8452
  138.7 179.8 %all-gather.8.cloned.1.call-start = ((), (), s32[]{:S(2)}) async-start(), calls=%async_computation.2 | async-start | bytes 3244032 | tf_op jit(solution)/shard_map/all_gather | solution.py:80
  139.6 220.6 %all-reduce.7.cloned.1.call-start = ((), (), s32[]{:S(2)}) async-start(), calls=%async_computation.4 | async-start | bytes 2097152 | tf_op jit(solution)/shard_map/psum | solution.py:89
  197.4 121.0 %copy-start.10 = (f32[704]{0:T(1024)S(1)}, f32[704]{0:T(1024)}, u32[]{:S(2)}) copy-start(f32[704]{0:T(1024)} %param.34) | copy-start | bytes 8452
Sparse Core Ops, SparseCore 0:
  137.1 33.7 all-reduce.4
  325.6 34.4 all-reduce.6
Sparse Core Ops, SparseCore 1:
  139.5 57.9 all-gather.5
  199.3 58.5 all-gather.9
  259.9 58.5 all-gather.7
where the time goes:
time: 371 us; the launch traced here: 370 us
  waiting for transfers between devices  192 us (52%)
  blocking collectives  139 us (37%)
  between operations  15.2 us (4%)
  matrix products  12.4 us (3%)
  other arithmetic  11.4 us (3%)
    all_gather x1, waiting for transfers between devices, body(): lax.all_gather(mlp_shards[1], 'fs', axis=0, tiled=True)  60.5 us
    all_gather x1, waiting for transfers between devices, body(): lax.all_gather(mlp_shards[2], 'fs', axis=0, tiled=True)  57.6 us
    psum x1, waiting for transfers between devices, body(): lax.psum(mlp_term.astype(jnp.bfloat16), 'tp').astype(jnp.float32)  34.6 us
    all_gather x1, blocking collectives, body(): lax.all_gather(value_proj.astype(jnp.bfloat16), 'fs', axis=0, tiled=True)  33 us
    all_gather x1, blocking collectives, body(): lax.all_gather(gate_proj.astype(jnp.bfloat16), 'fs', axis=0, tiled=True)  31.4 us
    all_gather x1, blocking collectives, body(): lax.all_gather(out_proj.astype(jnp.bfloat16), 'fs', axis=0, tiled=True)  31.3 us
    all_gather x1, waiting for transfers between devices, body(): lax.all_gather(mlp_shards[0], 'fs', axis=0, tiled=True)  24.8 us
    all_gather x1, blocking collectives, body(): lax.all_gather(out_scale, 'fs', axis=0, tiled=True)  20.7 us
  transfers between devices with their start and end apart: 5, of which 5 were waited for; matrix products, arithmetic and copies ran while one was open for 2% of the time, Pallas kernels for 0%

commit v1 on v0

--- a/solution.py
+++ b/solution.py
@@ -1,6 +1,10 @@
+import functools
+
 import jax
 import jax.numpy as jnp
 from jax import lax
+from jax.experimental import pallas as pl
+from jax.experimental.pallas import tpu as pltpu
 from jax.sharding import PartitionSpec as P
 
 
@@ -91,30 +95,429 @@
     )
 
 
+MESH = pl.DeviceIdType.MESH
+LANES = 128
+Y = 2
+CORES = 2
+
+
+def nearest_order(z, extent):
+    picks = []
+    for k in range(extent):
+        pick = jnp.int32(0)
+        for at in range(extent):
+            order = sorted(range(extent), key=lambda v: (abs(v - at), v))
+            pick = jnp.where(z == at, order[k], pick)
+        picks.append(pick)
+    return picks
+
+
+def layer_kernel(
+    Z,
+    hidden, mix_gain, value_p, gate_p, out_p, value_s, gate_s, out_s, taps_ref,
+    norm_gain, norm_shift, mlp_gain, mgate, mup, mdown, mgate_s, mup_s, mdown_s,
+    result,
+    vg, ow, gu, dn, normed, pad, mid, acc, hid, stat_out, stat_in, stat_t,
+    core_out, core_in, x_out, x_in,
+    g_send, g_recv, s_send, s_recv, c_send, c_recv, x_send, x_recv, f_send, f_recv,
+):
+    f32, bf16 = jnp.float32, jnp.bfloat16
+    fs, tp = lax.axis_index("fs"), lax.axis_index("tp")
+    z, y = fs // Y, lax.rem(fs, Y)
+    x, core = tp // CORES, lax.rem(tp, CORES)
+    yo = 1 - y
+    me = (fs, tp)
+    up, down = (fs + Y, tp), (fs - Y, tp)
+    across = (z * Y + yo, tp)
+    core_peer = (fs, x * CORES + 1 - core)
+    x_peer = (fs, (1 - x) * CORES + core)
+    diag_peer = (fs, (1 - x) * CORES + 1 - core)
+    has_up, has_down = z < Z - 1, z > 0
+
+    rows, width = hidden.shape
+    nblk = Z * Y
+    blk = width // nblk
+    ch = value_p.shape[1]
+    hu = mgate.shape[1]
+
+    vg[fs, :, :ch] = value_p[...].astype(bf16)
+    vg[fs, :, ch:] = gate_p[...].astype(bf16)
+    scale_col = jnp.broadcast_to(out_s[...], (LANES, blk)).T
+    ow[fs] = (out_p[...].astype(bf16).astype(f32) * scale_col[:, :1]).astype(bf16)
+
+    barrier = pltpu.get_barrier_semaphore()
+
+    def greet(peer):
+        pl.semaphore_signal(barrier, inc=1, device_id=peer, device_id_type=MESH)
+
+    for peer in (across, core_peer, x_peer, diag_peer):
+        greet(peer)
+
+    @pl.when(has_up)
+    def _():
+        greet(up)
+
+    @pl.when(has_down)
+    def _():
+        greet(down)
+
+    pl.semaphore_wait(barrier, 4 + has_up.astype(jnp.int32) + has_down.astype(jnp.int32))
+
+    half = blk // 2
+    quarter = blk // 4
+    pieces = [(vg, None), (ow, None)]
+    pieces += [(gu, (r * quarter, quarter)) for r in range(4)]
+    pieces += [(dn, (r * quarter, quarter)) for r in range(2)]
+    crossed = (3,)
+
+    def slot(p, at):
+        ref, cut = pieces[p]
+        return ref.at[at] if cut is None else ref.at[at, pl.ds(*cut)]
+
+    def copy(p, at, peer, way):
+        return pltpu.make_async_remote_copy(
+            src_ref=slot(p, at), dst_ref=slot(p, at),
+            send_sem=g_send.at[p, at, way], recv_sem=g_recv.at[p, at],
+            device_id=peer, device_id_type=MESH,
+        )
+
+    sent = []
+
+    def start(p, at, peer, way, cond=None):
+        if cond is None:
+            copy(p, at, peer, way).start()
+        else:
+            @pl.when(cond)
+            def _():
+                copy(p, at, peer, way).start()
+        sent.append((p, at, peer, way, cond))
+
+    def own(p):
+        start(p, fs, up, 0, has_up)
+        start(p, fs, down, 1, has_down)
+        start(p, fs, across, 2)
+
+    def arrived(p, at):
+        copy(p, at, across, 2).wait_recv()
+
+    def own_crossed(p):
+        at = z * Y + yo
+        arrived(p, at)
+        start(p, at, up, 0, has_up)
+        start(p, at, down, 1, has_down)
+
+    def relay(p, s):
+        lanes = (y, yo) if p in crossed else (y,)
+        for lane in lanes:
+            below, above = (z - s) * Y + lane, (z + s) * Y + lane
+            ok_b, ok_a = z - s >= 0, z + s < Z
+
+            @pl.when(ok_b)
+            def _(below=below):
+                arrived(p, below)
+
+            start(p, below, up, 0, jnp.logical_and(ok_b, has_up))
+            if p not in crossed:
+                start(p, below, across, 2, ok_b)
+
+            @pl.when(ok_a)
+            def _(above=above):
+                arrived(p, above)
+
+            start(p, above, down, 1, jnp.logical_and(ok_a, has_down))
+            if p not in crossed:
+                start(p, above, across, 2, ok_a)
+
+    def finish(p, zz=None):
+        if p not in crossed:
+            for at in range(Z) if zz is None else (zz,):
+                arrived(p, at * Y + yo)
+
+    def wave(t):
+        q0, count = 2, len(pieces) - 2
+        if t < count:
+            own(q0 + t)
+        if 0 <= t - 1 < count:
+            if q0 + t - 1 in crossed:
+                own_crossed(q0 + t - 1)
+        for s in range(1, Z):
+            if 0 <= t - s < count:
+                relay(q0 + t - s, s)
+
+    own(0)
+    own(1)
+
+    gu[fs, :, :hu] = mgate[...].astype(bf16)
+    gu[fs, :, hu:] = mup[...].astype(bf16)
+    scale_col = jnp.broadcast_to(mdown_s[...], (LANES, blk)).T
+    folded = (mdown[...].astype(bf16).astype(f32) * scale_col[:, :1]).astype(bf16)
+    dn[fs, :, :hu] = folded[:half]
+    dn[fs, :, hu:] = folded[half:]
+
+    relay(0, 1)
+    relay(1, 1)
+
+    h = hidden[...].astype(f32)
+    norm = lax.rsqrt(jnp.mean(h * h, axis=-1, keepdims=True) + 1e-06)
+    for b in range(nblk):
+        cols = slice(b * blk, (b + 1) * blk)
+        normed[b] = (hidden[:, cols].astype(f32) * norm * mix_gain[:, cols]).astype(bf16)
+
+    for s in range(2, Z):
+        relay(0, s)
+        relay(1, s)
+    wave(0)
+    finish(0)
+
+    pre = jnp.zeros((rows, 2 * ch), f32)
+    for b in range(nblk):
+        pre += jnp.dot(normed[b], vg[b], preferred_element_type=f32)
+    glu = pre[:, :ch] * value_s[...] * jax.nn.sigmoid(pre[:, ch:] * gate_s[...])
+    ntaps = taps_ref.shape[0]
+    lead = pad.shape[0] - rows
+    pad[pl.ds(0, lead)] = jnp.zeros((lead, ch), f32)
+    pad[pl.ds(lead, rows)] = glu
+    taps = taps_ref[...].astype(f32)
+    conved = jnp.zeros((rows, ch), f32)
+    for j in range(ntaps):
+        conved += pad[pl.ds(lead - ntaps + 1 + j, rows)] * taps[j : j + 1]
+    lane = lax.broadcasted_iota(jnp.int32, (rows, LANES), 1)
+    packed = jnp.where(
+        lane == 0,
+        jnp.sum(conved, axis=1, keepdims=True),
+        jnp.sum(conved * conved, axis=1, keepdims=True),
+    )
+    stat_t[...] = packed.T
+    stat_out[...] = stat_t[:8]
+
+    def stat_copy(k, peer):
+        return pltpu.make_async_remote_copy(
+            src_ref=stat_out, dst_ref=stat_in.at[k],
+            send_sem=s_send.at[k], recv_sem=s_recv.at[k],
+            device_id=peer, device_id_type=MESH,
+        )
+
+    stats = [stat_copy(k, p) for k, p in enumerate((core_peer, x_peer, diag_peer))]
+    for c in stats:
+        c.start()
+    wave(1)
+    for c in stats:
+        c.wait()
+    stat_t[pl.ds(0, 8)] = stat_out[...] + stat_in[0] + stat_in[1] + stat_in[2]
+    columns = stat_t[...].T
+    channels = ch * CORES * 2
+    mean = columns[:, 0:1] / channels
+    var = columns[:, 1:2] / channels - mean * mean
+    a = (conved - mean) * lax.rsqrt(var + 1e-05) * norm_gain[...] + norm_shift[...]
+    act = (a * jax.nn.sigmoid(a)).astype(bf16)
+    finish(1)
+
+    order = nearest_order(z, Z)
+    mine, theirs = lax.rem(y + core, Y), lax.rem(y + 1 - core, Y)
+
+    def core_copy(u, k):
+        return pltpu.make_async_remote_copy(
+            src_ref=core_out.at[u, k], dst_ref=core_in.at[u, k],
+            send_sem=c_send.at[u, k], recv_sem=c_recv.at[u, k],
+            device_id=core_peer, device_id_type=MESH,
+        )
+
+    def x_copy(u, k):
+        return pltpu.make_async_remote_copy(
+            src_ref=x_out.at[u, k], dst_ref=x_in.at[u, k],
+            send_sem=x_send.at[u, k], recv_sem=x_recv.at[u, k],
+            device_id=x_peer, device_id_type=MESH,
+        )
+
+    def final_copy(u, ref, at):
+        return pltpu.make_async_remote_copy(
+            src_ref=ref.at[at], dst_ref=ref.at[at],
+            send_sem=f_send.at[u, at], recv_sem=f_recv.at[u, at],
+            device_id=core_peer, device_id_type=MESH,
+        )
+
+    def conv_term(b):
+        return lax.dot_general(act, ow[b], (((1,), (1,)), ((), ())), preferred_element_type=f32)
+
+    for k in range(Z):
+        core_out[0, k] = conv_term(order[k] * Y + theirs).astype(bf16)
+        core_copy(0, k).start()
+    wave(2)
+    for k in range(Z):
+        term = conv_term(order[k] * Y + mine)
+        core_copy(0, k).wait_recv()
+        x_out[0, k] = (term + core_in[0, k].astype(f32)).astype(bf16)
+        x_copy(0, k).start()
+    wave(3)
+    for k in range(Z):
+        b = order[k] * Y + mine
+        x_copy(0, k).wait_recv()
+        cols = pl.ds(pl.multiple_of(b * blk, blk), blk)
+        total = x_out[0, k].astype(f32) + x_in[0, k].astype(f32)
+        mid[b] = (hidden[:, cols].astype(f32) + total).astype(bf16)
+        final_copy(0, mid, b).start()
+    wave(4)
+    for k in range(Z):
+        final_copy(0, mid, order[k] * Y + theirs).wait_recv()
+
+    total = jnp.zeros((rows, 1), f32)
+    for b in range(nblk):
+        m = mid[b].astype(f32)
+        total += jnp.sum(m * m, axis=-1, keepdims=True)
+    norm = lax.rsqrt(total / width + 1e-06)
+    for b in range(nblk):
+        cols = slice(b * blk, (b + 1) * blk)
+        normed[b] = (mid[b].astype(f32) * norm * mlp_gain[:, cols]).astype(bf16)
+    for t in range(5, len(pieces) - 2 + Z - 1):
+        wave(t)
+
+    for p in range(2, 6):
+        finish(p)
+    acc[...] = jnp.dot(normed[0], gu[0], preferred_element_type=f32)
+
+    def step(b, carry):
+        acc[...] += jnp.dot(normed[b], gu[b], preferred_element_type=f32)
+        return carry
+
+    lax.fori_loop(1, nblk, step, 0)
+    gate = acc[:, :hu] * mgate_s[...]
+    up_v = acc[:, hu:] * mup_s[...]
+    act2 = (gate * jax.nn.sigmoid(gate) * up_v).astype(bf16)
+    zero = jnp.zeros_like(act2)
+    hid[0, :, :hu] = act2
+    hid[0, :, hu:] = zero
+    hid[1, :, :hu] = zero
+    hid[1, :, hu:] = act2
+
+    dims = (((1,), (1,)), ((), ()))
+
+    def mlp_term(b):
+        return [
+            lax.dot_general(hid[i], dn[b], dims, preferred_element_type=f32) for i in range(2)
+        ]
+
+    def send_theirs(k):
+        for i, t in enumerate(mlp_term(order[k] * Y + theirs)):
+            core_out[1, k, :, i * half : (i + 1) * half] = t.astype(bf16)
+        core_copy(1, k).start()
+
+    def send_mine(k):
+        terms = mlp_term(order[k] * Y + mine)
+        core_copy(1, k).wait_recv()
+        for i, t in enumerate(terms):
+            cols = slice(i * half, (i + 1) * half)
+            x_out[1, k, :, cols] = (t + core_in[1, k, :, cols].astype(f32)).astype(bf16)
+        x_copy(1, k).start()
+
+    def send_final(k):
+        b = order[k] * Y + mine
+        x_copy(1, k).wait_recv()
+        total = x_out[1, k].astype(f32) + x_in[1, k].astype(f32)
+        result[b] = (mid[b].astype(f32) + total).astype(bf16)
+        final_copy(1, result, b).start()
+
+    for k in range(Z):
+        finish(6, order[k])
+        finish(7, order[k])
+        send_theirs(k)
+        send_mine(k)
+        if k:
+            send_final(k - 1)
+    send_final(Z - 1)
+    for k in range(Z):
+        final_copy(1, result, order[k] * Y + theirs).wait_recv()
+
+    for p, at, peer, way, cond in sent:
+        if cond is None:
+            copy(p, at, peer, way).wait_send()
+        else:
+            @pl.when(cond)
+            def _(p=p, at=at, peer=peer, way=way):
+                copy(p, at, peer, way).wait_send()
+    for u, ref in ((0, mid), (1, result)):
+        for k in range(Z):
+            core_copy(u, k).wait_send()
+            x_copy(u, k).wait_send()
+            final_copy(u, ref, order[k] * Y + mine).wait_send()
+
+
+def kernel_body(*args):
+    n_fs = lax.axis_size("fs")
+    Z = n_fs // Y
+    hidden, value_p, taps, mgate = args[0], args[2], args[8], args[12]
+    rows, width = hidden.shape
+    blk, ch, hu = width // n_fs, value_p.shape[1], mgate.shape[1]
+    args = [a.reshape(1, -1) if a.ndim == 1 else a for a in args]
+    lead = -(-(taps.shape[0] - 1) // 8) * 8
+    bf16, f32 = jnp.bfloat16, jnp.float32
+    dma = pltpu.SemaphoreType.DMA
+    n_pieces = 8
+    out = pl.pallas_call(
+        functools.partial(layer_kernel, Z),
+        out_shape=jax.ShapeDtypeStruct((n_fs, rows, blk), bf16),
+        in_specs=[pl.BlockSpec(memory_space=pltpu.VMEM)] * len(args),
+        out_specs=pl.BlockSpec(memory_space=pltpu.VMEM),
+        scratch_shapes=[
+            pltpu.VMEM((n_fs, blk, 2 * ch), bf16),
+            pltpu.VMEM((n_fs, blk, ch), bf16),
+            pltpu.VMEM((n_fs, blk, 2 * hu), bf16),
+            pltpu.VMEM((n_fs, blk // 2, 2 * hu), bf16),
+            pltpu.VMEM((n_fs, rows, blk), bf16),
+            pltpu.VMEM((lead + rows, ch), f32),
+            pltpu.VMEM((n_fs, rows, blk), bf16),
+            pltpu.VMEM((rows, 2 * hu), f32),
+            pltpu.VMEM((2, rows, 2 * hu), bf16),
+            pltpu.VMEM((8, rows), f32),
+            pltpu.VMEM((3, 8, rows), f32),
+            pltpu.VMEM((LANES, rows), f32),
+            pltpu.VMEM((2, Z, rows, blk), bf16),
+            pltpu.VMEM((2, Z, rows, blk), bf16),
+            pltpu.VMEM((2, Z, rows, blk), bf16),
+            pltpu.VMEM((2, Z, rows, blk), bf16),
+            dma((n_pieces, n_fs, 3)),
+            dma((n_pieces, n_fs)),
+            dma((3,)),
+            dma((3,)),
+            dma((2, Z)),
+            dma((2, Z)),
+            dma((2, Z)),
+            dma((2, Z)),
+            dma((2, n_fs)),
+            dma((2, n_fs)),
+        ],
+        compiler_params=pltpu.CompilerParams(
+            collective_id=0, has_side_effects=True, vmem_limit_bytes=56 * 1024 * 1024
+        ),
+    )(*args)
+    return out.transpose(1, 0, 2).reshape(rows, width)
+
+
+def fits(mesh, args):
+    n_fs, n_tp = mesh.shape["fs"], mesh.shape["tp"]
+    ch, hu = args[2].shape[1] // n_tp, args[12].shape[1] // n_tp
+    blk = args[0].shape[1] // n_fs
+    return (
+        n_fs % Y == 0
+        and n_tp == 2 * CORES
+        and ch % LANES == 0
+        and (2 * hu) % LANES == 0
+        and blk % (2 * LANES) == 0
+        and n_fs <= 8
+    )
+
+
+SPECS = (
+    P("fs", None), P(), P("fs", "tp"), P("fs", "tp"), P("fs", "tp"), P("tp"), P("tp"),
+    P("fs"), P(None, "tp"), P("tp"), P("tp"), P(), P("fs", "tp"), P("fs", "tp"),
+    P("fs", "tp"), P("tp"), P("tp"), P("fs"),
+)
+
+
 def solution(mesh):
-    return jax.shard_map(
-        body,
-        mesh=mesh,
-        in_specs=(
-            P("fs", None),
-            P(),
-            P("fs", "tp"),
-            P("fs", "tp"),
-            P("fs", "tp"),
-            P("tp"),
-            P("tp"),
-            P("fs"),
-            P(None, "tp"),
-            P("tp"),
-            P("tp"),
-            P(),
-            P("fs", "tp"),
-            P("fs", "tp"),
-            P("fs", "tp"),
-            P("tp"),
-            P("tp"),
-            P("fs"),
-        ),
-        out_specs=P("fs", None),
-        check_vma=False,
-    )
+    def run(*args):
+        return jax.shard_map(
+            kernel_body if fits(mesh, args) else body,
+            mesh=mesh, in_specs=SPECS, out_specs=P("fs", None), check_vma=False,
+        )(*args)
+
+    return run

time: 371 us -> 138 us (0.37)
  waiting for transfers between devices: 192 us -> 0 us
  blocking collectives: 139 us -> 0 us
  Pallas kernels: 0 us -> 128 us
  between operations: 15.2 us -> 0.02 us
  matrix products: 12.4 us -> 0 us
  other arithmetic: 11.4 us -> 0 us
  local copies, waits for them, and re-layouts: 0.09 us -> 9.44 us
    all_gather x3 -> x0, waiting for transfers between devices: 143 us -> none  [the longest x1 60.5 us: body(): lax.all_gather(mlp_shards[1], 'fs', axis=0, tiled=True)]
    all_gather x5 -> x0, blocking collectives: 133 us -> none  [the longest x1 33 us: body(): lax.all_gather(value_proj.astype(jnp.bfloat16), 'fs', axis=0, tiled=True)]
    pallas_call x0 -> x1, Pallas kernels: none -> 128 us  [kernel_body(): pl.pallas_call(functools.partial(layer_kernel, Z), out_shape=jax.ShapeDty...]
    psum x2 -> x0, waiting for transfers between devices: 49.3 us -> none  [the longest x1 34.6 us: body(): lax.psum(mlp_term.astype(jnp.bfloat16), 'tp').astype(jnp.float32)]
    dot_general x5 -> x0, matrix products: 12.4 us -> none  [the longest x2 8.52 us: contract_last(): lax.dot_general(left, right, (((1,), (1,)), ((), ())), preferred_element_...]
    convert_element_type x8 -> x0, other arithmetic: 7.58 us -> none  [the longest x1 2.58 us: body(): (middle_f + lax.psum(mlp_term.astype(jnp.bfloat16), 'tp').astype(jnp.floa...]
    psum x1 -> x0, blocking collectives: 5.66 us -> none  [body(): lax.psum((jnp.sum(conved, axis=1), jnp.sum(conved * conved, axis=1)), 'tp')]
    unnamed x30 -> x11, local copies, waits for them, and re-layouts: 0.07 us -> 5.35 us
  transfers between devices with their start and end apart: 5 -> 0, of which waited for: 5 -> 0; matrix products, arithmetic and copies ran while one was open for 2% -> 0% of each run, Pallas kernels for 0% -> 0%
where the time goes in v1:
time: 138 us; the launch traced here: 137 us
  Pallas kernels  128 us (93%)
  local copies, waits for them, and re-layouts  9.44 us (7%)
    pallas_call x1, Pallas kernels, kernel_body(): pl.pallas_call(functools.partial(layer_kernel, Z), out_shape=jax.ShapeDty...  128 us
    unnamed x11, local copies, waits for them, and re-layouts  5.35 us

profile of v1, /device:TPU:0, one launch (start us, length us, event | category | flops | bytes accessed | tf_op | source)
XLA Modules:
  0.0 137.4 jit_solution(7335402089244287666)
XLA Ops:
  0.0 0.0 copy-start.2
  0.0 0.0 copy-start.3
  0.0 0.7 copy-done.2
  0.7 0.6 reshape.40.mgate_s
  1.3 0.0 copy-done.3
  1.3 0.6 reshape.41.mup_s
  1.9 0.0 copy-start
  1.9 2.3 %copy.22.mgate = f32[256,704]{1,0:T(8,128)} copy(f32[256,704]{0,1:T(8,128)} %param.30) | data formatting | bytes 1441792 | tf_op args[12]
  4.2 0.0 copy-done
  4.2 0.0 copy-start.1
  4.2 1.2 copy.23.mup
  5.4 0.0 copy-done.1
  5.4 1.1 copy.24.mdown
  6.5 127.9 %shard_map.172 = bf16[8,256,256]{2,1,0:T(8,128)(2,1)} custom-call(bf16[256,2048]{1,0:T(8,128)(2,1)} %hidden.1, f32[1,2048]{1,0:T(1,128)} %bitcast.12, f32[256,128]{1,0:T(8,128)} %value_p.1, f32[256,128]{1,0:T(8,128)} %gate_p.1, f32[256,128]{1,0:T(8,128)} %out_p.1, f32[1,128]{1,0:T(1,128)} %bitcast.16, f32[1,128]{1,0:T(1,128)} %bitcast.17, ...), custom_call_target="tpu_custom_call" | custom-call | tf_op jit(solution)/shard_map/pallas_call | solution.py:455
  134.5 1.5 %copy.25 = bf16[256,8,256]{0,2,1:T(8,128)(2,1)S(1)} copy(bf16[256,8,256]{2,0,1:T(8,128)(2,1)} %bitcast.11) | data formatting | bytes 2097152 | tf_op jit(solution)/shard_map/transpose | solution.py:492
  136.0 1.4 %copy.26 = bf16[256,2048]{1,0:T(8,128)(2,1)} copy(bf16[256,2048]{0,1:T(8,128)(2,1)S(1)} %bitcast.10) | data formatting | bytes 2097152 | tf_op jit(solution)/shard_map/reshape | solution.py:492
Async XLA Ops:
  0.0 0.7 copy-start.2
  0.0 1.3 copy-start.3
  1.9 2.3 %copy-start = (f32[256,704]{0,1:T(8,128)S(1)}, f32[256,704]{0,1:T(8,128)}, u32[]{:S(2)}) copy-start(f32[256,704]{0,1:T(8,128)} %param.31) | copy-start | bytes 2162692
  4.2 1.2 copy-start.1

commit v2 on v1

--- a/solution.py
+++ b/solution.py
@@ -99,6 +99,9 @@
 LANES = 128
 Y = 2
 CORES = 2
+ROW = 1024
+AHEAD_Y = 3
+AHEAD_Z = 2
 
 
 def nearest_order(z, extent):
@@ -114,12 +117,14 @@
 
 def layer_kernel(
     Z,
-    hidden, mix_gain, value_p, gate_p, out_p, value_s, gate_s, out_s, taps_ref,
-    norm_gain, norm_shift, mlp_gain, mgate, mup, mdown, mgate_s, mup_s, mdown_s,
-    result,
-    vg, ow, gu, dn, normed, pad, mid, acc, hid, stat_out, stat_in, stat_t,
+    hidden_hbm, mix_gain, value_p, gate_p, out_p, value_s, gate_s, out_s, taps_ref,
+    norm_gain, norm_shift, mlp_gain, mgate_hbm, mup_hbm, mdown_hbm, mid_s, mdown_s,
+    result_hbm,
+    hidden, mgate, mup, mdown, result,
+    vg, ow, gu, dn, normed, pad, mid, acc, acc_up, stat_out, stat_in, stat_t,
     core_out, core_in, x_out, x_in,
     g_send, g_recv, s_send, s_recv, c_send, c_recv, x_send, x_recv, f_send, f_recv,
+    l_sem, o_sem,
 ):
     f32, bf16 = jnp.float32, jnp.bfloat16
     fs, tp = lax.axis_index("fs"), lax.axis_index("tp")
@@ -138,7 +143,15 @@
     nblk = Z * Y
     blk = width // nblk
     ch = value_p.shape[1]
-    hu = mgate.shape[1]
+    hu = mgate.shape[0]
+    fetches = [
+        pltpu.make_async_copy(src, dst, l_sem.at[i])
+        for i, (src, dst) in enumerate(
+            ((hidden_hbm, hidden), (mgate_hbm, mgate), (mup_hbm, mup), (mdown_hbm, mdown))
+        )
+    ]
+    for f in fetches:
+        f.start()
 
     vg[fs, :, :ch] = value_p[...].astype(bf16)
     vg[fs, :, ch:] = gate_p[...].astype(bf16)
@@ -163,8 +176,7 @@
 
     pl.semaphore_wait(barrier, 4 + has_up.astype(jnp.int32) + has_down.astype(jnp.int32))
 
-    half = blk // 2
-    quarter = blk // 4
+    quarter = hu // 2
     pieces = [(vg, None), (ow, None)]
     pieces += [(gu, (r * quarter, quarter)) for r in range(4)]
     pieces += [(dn, (r * quarter, quarter)) for r in range(2)]
@@ -192,10 +204,16 @@
                 copy(p, at, peer, way).start()
         sent.append((p, at, peer, way, cond))
 
-    def own(p):
+    def own_z(p):
         start(p, fs, up, 0, has_up)
         start(p, fs, down, 1, has_down)
+
+    def own_y(p):
         start(p, fs, across, 2)
+
+    def own(p):
+        own_y(p)
+        own_z(p)
 
     def arrived(p, at):
         copy(p, at, across, 2).wait_recv()
@@ -235,8 +253,12 @@
 
     def wave(t):
         q0, count = 2, len(pieces) - 2
-        if t < count:
-            own(q0 + t)
+        for q in range(AHEAD_Y + 1) if t == 0 else (t + AHEAD_Y,):
+            if q < count:
+                own_y(q0 + q)
+        for q in range(AHEAD_Z + 1) if t == 0 else (t + AHEAD_Z,):
+            if q < count:
+                own_z(q0 + q)
         if 0 <= t - 1 < count:
             if q0 + t - 1 in crossed:
                 own_crossed(q0 + t - 1)
@@ -247,12 +269,11 @@
     own(0)
     own(1)
 
-    gu[fs, :, :hu] = mgate[...].astype(bf16)
-    gu[fs, :, hu:] = mup[...].astype(bf16)
-    scale_col = jnp.broadcast_to(mdown_s[...], (LANES, blk)).T
-    folded = (mdown[...].astype(bf16).astype(f32) * scale_col[:, :1]).astype(bf16)
-    dn[fs, :, :hu] = folded[:half]
-    dn[fs, :, hu:] = folded[half:]
+    for f in fetches:
+        f.wait()
+    gu[fs, :hu] = mgate[...].astype(bf16)
+    gu[fs, hu:] = mup[...].astype(bf16)
+    dn[fs] = (mdown[...].astype(bf16).astype(f32) * mdown_s[...]).astype(bf16)
 
     relay(0, 1)
     relay(1, 1)
@@ -373,40 +394,39 @@
 
     for p in range(2, 6):
         finish(p)
-    acc[...] = jnp.dot(normed[0], gu[0], preferred_element_type=f32)
+    dims = (((1,), (1,)), ((), ()))
+
+    def gate_up(b):
+        return (
+            lax.dot_general(normed[b], gu[b, :hu], dims, preferred_element_type=f32),
+            lax.dot_general(normed[b], gu[b, hu:], dims, preferred_element_type=f32),
+        )
+
+    acc[...], acc_up[...] = gate_up(0)
 
     def step(b, carry):
-        acc[...] += jnp.dot(normed[b], gu[b], preferred_element_type=f32)
+        g, u = gate_up(b)
+        acc[...] += g
+        acc_up[...] += u
         return carry
 
     lax.fori_loop(1, nblk, step, 0)
-    gate = acc[:, :hu] * mgate_s[...]
-    up_v = acc[:, hu:] * mup_s[...]
+    gate = acc[...] * mid_s[:, :hu]
+    second = mid_s.shape[1] // 2
+    up_v = acc_up[...] * mid_s[:, second : second + hu]
     act2 = (gate * jax.nn.sigmoid(gate) * up_v).astype(bf16)
-    zero = jnp.zeros_like(act2)
-    hid[0, :, :hu] = act2
-    hid[0, :, hu:] = zero
-    hid[1, :, :hu] = zero
-    hid[1, :, hu:] = act2
-
-    dims = (((1,), (1,)), ((), ()))
 
     def mlp_term(b):
-        return [
-            lax.dot_general(hid[i], dn[b], dims, preferred_element_type=f32) for i in range(2)
-        ]
+        return jnp.dot(act2, dn[b], preferred_element_type=f32)
 
     def send_theirs(k):
-        for i, t in enumerate(mlp_term(order[k] * Y + theirs)):
-            core_out[1, k, :, i * half : (i + 1) * half] = t.astype(bf16)
+        core_out[1, k] = mlp_term(order[k] * Y + theirs).astype(bf16)
         core_copy(1, k).start()
 
     def send_mine(k):
-        terms = mlp_term(order[k] * Y + mine)
+        term = mlp_term(order[k] * Y + mine)
         core_copy(1, k).wait_recv()
-        for i, t in enumerate(terms):
-            cols = slice(i * half, (i + 1) * half)
-            x_out[1, k, :, cols] = (t + core_in[1, k, :, cols].astype(f32)).astype(bf16)
+        x_out[1, k] = (term + core_in[1, k].astype(f32)).astype(bf16)
         x_copy(1, k).start()
 
     def send_final(k):
@@ -415,6 +435,11 @@
         total = x_out[1, k].astype(f32) + x_in[1, k].astype(f32)
         result[b] = (mid[b].astype(f32) + total).astype(bf16)
         final_copy(1, result, b).start()
+        out_copy(b).start()
+
+    def out_copy(b):
+        cols = pl.ds(pl.multiple_of(b * blk, blk), blk)
+        return pltpu.make_async_copy(result.at[b], result_hbm.at[:, cols], o_sem.at[b])
 
     for k in range(Z):
         finish(6, order[k])
@@ -425,7 +450,11 @@
             send_final(k - 1)
     send_final(Z - 1)
     for k in range(Z):
-        final_copy(1, result, order[k] * Y + theirs).wait_recv()
+        b = order[k] * Y + theirs
+        final_copy(1, result, b).wait_recv()
+        out_copy(b).start()
+    for b in range(nblk):
+        out_copy(b).wait()
 
     for p, at, peer, way, cond in sent:
         if cond is None:
@@ -446,6 +475,11 @@
     Z = n_fs // Y
     hidden, value_p, taps, mgate = args[0], args[2], args[8], args[12]
     rows, width = hidden.shape
+    args = list(args)
+    for i in (12, 13, 14):
+        args[i] = args[i].T
+    gap = jnp.zeros((-args[15].shape[0] % ROW,), jnp.float32)
+    args[15:17] = [jnp.concatenate([args[15], gap, args[16], gap])]
     blk, ch, hu = width // n_fs, value_p.shape[1], mgate.shape[1]
     args = [a.reshape(1, -1) if a.ndim == 1 else a for a in args]
     lead = -(-(taps.shape[0] - 1) // 8) * 8
@@ -454,19 +488,27 @@
     n_pieces = 8
     out = pl.pallas_call(
         functools.partial(layer_kernel, Z),
-        out_shape=jax.ShapeDtypeStruct((n_fs, rows, blk), bf16),
-        in_specs=[pl.BlockSpec(memory_space=pltpu.VMEM)] * len(args),
-        out_specs=pl.BlockSpec(memory_space=pltpu.VMEM),
+        out_shape=jax.ShapeDtypeStruct((rows, width), bf16),
+        in_specs=[
+            pl.BlockSpec(memory_space=pl.ANY if i in (0, 12, 13, 14) else pltpu.VMEM)
+            for i in range(len(args))
+        ],
+        out_specs=pl.BlockSpec(memory_space=pl.ANY),
         scratch_shapes=[
+            pltpu.VMEM((rows, width), bf16),
+            pltpu.VMEM((hu, blk), f32),
+            pltpu.VMEM((hu, blk), f32),
+            pltpu.VMEM((hu, blk), f32),
+            pltpu.VMEM((n_fs, rows, blk), bf16),
             pltpu.VMEM((n_fs, blk, 2 * ch), bf16),
             pltpu.VMEM((n_fs, blk, ch), bf16),
-            pltpu.VMEM((n_fs, blk, 2 * hu), bf16),
-            pltpu.VMEM((n_fs, blk // 2, 2 * hu), bf16),
+            pltpu.VMEM((n_fs, 2 * hu, blk), bf16),
+            pltpu.VMEM((n_fs, hu, blk), bf16),
             pltpu.VMEM((n_fs, rows, blk), bf16),
             pltpu.VMEM((lead + rows, ch), f32),
             pltpu.VMEM((n_fs, rows, blk), bf16),
-            pltpu.VMEM((rows, 2 * hu), f32),
-            pltpu.VMEM((2, rows, 2 * hu), bf16),
+            pltpu.VMEM((rows, hu), f32),
+            pltpu.VMEM((rows, hu), f32),
             pltpu.VMEM((8, rows), f32),
             pltpu.VMEM((3, 8, rows), f32),
             pltpu.VMEM((LANES, rows), f32),
@@ -484,12 +526,14 @@
             dma((2, Z)),
             dma((2, n_fs)),
             dma((2, n_fs)),
+            dma((4,)),
+            dma((n_fs,)),
         ],
         compiler_params=pltpu.CompilerParams(
             collective_id=0, has_side_effects=True, vmem_limit_bytes=56 * 1024 * 1024
         ),
     )(*args)
-    return out.transpose(1, 0, 2).reshape(rows, width)
+    return out
 
 
 def fits(mesh, args):
@@ -500,7 +544,7 @@
         n_fs % Y == 0
         and n_tp == 2 * CORES
         and ch % LANES == 0
-        and (2 * hu) % LANES == 0
+        and hu % 32 == 0
         and blk % (2 * LANES) == 0
         and n_fs <= 8
     )

time: 138 us -> 131 us (0.949)
  local copies, waits for them, and re-layouts: 9.44 us -> 3.68 us
  Pallas kernels: 128 us -> 126 us
    reshape x3 -> x0, local copies, waits for them, and re-layouts: 2.61 us -> none  [the longest x1 1.42 us: kernel_body(): return out.transpose(1, 0, 2).reshape(rows, width)]
    unnamed x11 -> x5, local copies, waits for them, and re-layouts: 5.35 us -> 3 us
    transpose x1 -> x0, local copies, waits for them, and re-layouts: 1.48 us -> none  [kernel_body(): return out.transpose(1, 0, 2).reshape(rows, width)]
    pallas_call x1, Pallas kernels: 128 us -> 126 us  [kernel_body(): pl.pallas_call(functools.partial(layer_kernel, Z), out_shape=jax.ShapeDty...]
where the time goes in v2:
time: 131 us; the launch traced here: 130 us
  Pallas kernels  126 us (96%)
  local copies, waits for them, and re-layouts  3.68 us (3%)
    pallas_call x1, Pallas kernels, kernel_body(): pl.pallas_call(functools.partial(layer_kernel, Z), out_shape=jax.ShapeDty...  126 us
    unnamed x5, local copies, waits for them, and re-layouts  3 us

profile of v2, /device:TPU:0, one launch (start us, length us, event | category | flops | bytes accessed | tf_op | source)
XLA Modules:
  0.0 130.2 jit_solution(478989542864308956)
XLA Ops:
  0.0 0.0 copy-start
  0.0 0.0 copy-start.1
  0.0 0.7 copy-done
  0.7 0.0 copy-done.1
  0.7 0.7 concatenate.3
  1.4 126.5 %shard_map.172 = bf16[256,2048]{1,0:T(8,128)(2,1)} custom-call(bf16[256,2048]{1,0:T(8,128)(2,1)} %hidden_hbm.1, f32[1,2048]{1,0:T(1,128)} %bitcast.16, f32[256,128]{1,0:T(8,128)} %value_p.1, f32[256,128]{1,0:T(8,128)} %gate_p.1, f32[256,128]{1,0:T(8,128)} %out_p.1, f32[1,128]{1,0:T(1,128)} %bitcast.20, f32[1,128]{1,0:T(1,128)} %bitcast.21, ...), custom_call_target="tpu_custom_call" | custom-call | tf_op jit(solution)/shard_map/pallas_call | solution.py:489
  127.9 2.3 %copy.20 = bf16[256,2048]{1,0:T(8,128)(2,1)} copy(bf16[256,2048]{1,0:T(8,128)(2,1)} %shard_map.172) | data formatting | bytes 2097152
  (1 shorter events, 0.0 us)
Async XLA Ops:
  0.0 0.7 copy-start
  0.0 0.7 copy-start.1

commit v3 on v2

--- a/solution.py
+++ b/solution.py
@@ -180,7 +180,7 @@
     pieces = [(vg, None), (ow, None)]
     pieces += [(gu, (r * quarter, quarter)) for r in range(4)]
     pieces += [(dn, (r * quarter, quarter)) for r in range(2)]
-    crossed = (3,)
+    crossed = (5,)
 
     def slot(p, at):
         ref, cut = pieces[p]
@@ -288,6 +288,8 @@
         relay(0, s)
         relay(1, s)
     wave(0)
+    wave(1)
+    wave(2)
     finish(0)
 
     pre = jnp.zeros((rows, 2 * ch), f32)
@@ -321,7 +323,7 @@
     stats = [stat_copy(k, p) for k, p in enumerate((core_peer, x_peer, diag_peer))]
     for c in stats:
         c.start()
-    wave(1)
+    wave(3)
     for c in stats:
         c.wait()
     stat_t[pl.ds(0, 8)] = stat_out[...] + stat_in[0] + stat_in[1] + stat_in[2]
@@ -363,13 +365,12 @@
     for k in range(Z):
         core_out[0, k] = conv_term(order[k] * Y + theirs).astype(bf16)
         core_copy(0, k).start()
-    wave(2)
     for k in range(Z):
         term = conv_term(order[k] * Y + mine)
         core_copy(0, k).wait_recv()
         x_out[0, k] = (term + core_in[0, k].astype(f32)).astype(bf16)
         x_copy(0, k).start()
-    wave(3)
+    wave(4)
     for k in range(Z):
         b = order[k] * Y + mine
         x_copy(0, k).wait_recv()
@@ -377,7 +378,7 @@
         total = x_out[0, k].astype(f32) + x_in[0, k].astype(f32)
         mid[b] = (hidden[:, cols].astype(f32) + total).astype(bf16)
         final_copy(0, mid, b).start()
-    wave(4)
+    wave(5)
     for k in range(Z):
         final_copy(0, mid, order[k] * Y + theirs).wait_recv()
 
@@ -389,7 +390,7 @@
     for b in range(nblk):
         cols = slice(b * blk, (b + 1) * blk)
         normed[b] = (mid[b].astype(f32) * norm * mlp_gain[:, cols]).astype(bf16)
-    for t in range(5, len(pieces) - 2 + Z - 1):
+    for t in range(6, len(pieces) - 2 + Z - 1):
         wave(t)
 
     for p in range(2, 6):

time: 131 us -> 129 us (0.985)
    pallas_call x1, Pallas kernels: 126 us -> 125 us  [kernel_body(): pl.pallas_call(functools.partial(layer_kernel, Z), out_shape=jax.ShapeDty...]
where the time goes in v3:
time: 129 us; the launch traced here: 128 us
  Pallas kernels  125 us (97%)
  local copies, waits for them, and re-layouts  3.68 us (3%)
    pallas_call x1, Pallas kernels, kernel_body(): pl.pallas_call(functools.partial(layer_kernel, Z), out_shape=jax.ShapeDty...  125 us
    unnamed x5, local copies, waits for them, and re-layouts  3 us

profile of v3, /device:TPU:0, one launch (start us, length us, event | category | flops | bytes accessed | tf_op | source)
XLA Modules:
  0.0 128.5 jit_solution(16458811010678729395)
XLA Ops:
  0.0 0.0 copy-start
  0.0 0.0 copy-start.1
  0.0 0.7 copy-done
  0.7 0.0 copy-done.1
  0.7 0.7 concatenate.3
  1.4 124.8 %shard_map.172 = bf16[256,2048]{1,0:T(8,128)(2,1)} custom-call(bf16[256,2048]{1,0:T(8,128)(2,1)} %hidden_hbm.1, f32[1,2048]{1,0:T(1,128)} %bitcast.16, f32[256,128]{1,0:T(8,128)} %value_p.1, f32[256,128]{1,0:T(8,128)} %gate_p.1, f32[256,128]{1,0:T(8,128)} %out_p.1, f32[1,128]{1,0:T(1,128)} %bitcast.20, f32[1,128]{1,0:T(1,128)} %bitcast.21, ...), custom_call_target="tpu_custom_call" | custom-call | tf_op jit(solution)/shard_map/pallas_call | solution.py:490
  126.2 2.3 %copy.20 = bf16[256,2048]{1,0:T(8,128)(2,1)} copy(bf16[256,2048]{1,0:T(8,128)(2,1)} %shard_map.172) | data formatting | bytes 2097152
  (1 shorter events, 0.0 us)
Async XLA Ops:
  0.0 0.7 copy-start
  0.0 0.7 copy-start.1
